TPU v7x, 32 devices: a whole 2x2x4 slice. The times are simulated.
32 devices in a mesh: sp: 4 (over z), fs: 4 (over y, x), tp: 2 (over core).
Axes of the slice: x: 2, y: 2, z: 4, core: 2. Of those that a mesh axis runs over, the one named last changes fastest.
Arguments:
- tokens: bfloat16 [1024, 2048], P(('sp', 'fs', 'tp')), may hold values from -6 to 6
- norm_gain: float32 [2048], replicated, may hold values from 0.1 to 1.9
- w_query: bfloat16 [2048, 2048], P(None, ('fs', 'tp')), may hold values from -0.9722718 to 0.9722718
- w_key: bfloat16 [2048, 512], P(None, 'fs'), may hold values from -0.77339804 to 0.77339804
- w_value: bfloat16 [2048, 512], P(None, 'fs'), may hold values from -0.125 to 0.125
- w_conv_value: bfloat16 [2048, 1024], P(None, ('fs', 'tp')), may hold values from -0.125 to 0.125
- w_conv_pre: bfloat16 [2048, 1024], P(None, ('fs', 'tp')), may hold values from -0.125 to 0.125
- w_conv_post: bfloat16 [2048, 1024], P(None, ('fs', 'tp')), may hold values from -0.125 to 0.125
- conv_taps: bfloat16 [3, 1024], replicated, may hold values from -3.5 to 3.5
- log_gate_cache: float32 [16, 1024], replicated, may hold values from -65 to 0, as said below
- w_out_conv: bfloat16 [1024, 2048], P(('fs', 'tp')), may hold values from -0.125 to 0.125
- w_out_attn: bfloat16 [2048, 2048], P(('fs', 'tp')), may hold values from -0.375 to 0.375
Outputs:
- mixed: bfloat16 [1024, 2048], P(('sp', 'fs', 'tp'))
Inputs may be any that keep to these rules, and one draw needn't show every extreme that they name: `log_gate_cache`: each row is a cumulative sum over positions of log forget gates, none of them positive.
All inputs are finite; a program needn't handle non-finite values.
Results may differ from a plain program's by a relative error of at most 0.014.
The roundings to bfloat16 on the way count: a program that leaves them out, or rounds other values in their place, can miss the bound.
Values may be sent and summed in bfloat16 or wider, within the bound.
A program may use at most 64 MiB of HBM per device.

v0:
```python
import jax
import jax.numpy as jnp
from jax import lax
from jax.sharding import PartitionSpec as P

epsilon = 1e-06
masked_score = -1e30


def passed_along(block, axis, distance):
    devices = range(lax.axis_size(axis))
    route = [(i - distance, i) for i in devices if i - distance in devices]
    return lax.ppermute(block, axis, route)


def shards(
    tokens,
    norm_gain,
    w_query,
    w_key,
    w_value,
    w_conv_value,
    w_conv_pre,
    w_conv_post,
    conv_taps,
    log_gate_cache,
    w_out_conv,
    w_out_attn,
):
    float_rows = tokens.astype(jnp.float32)
    scaled = float_rows * lax.rsqrt(
        jnp.mean(float_rows * float_rows, axis=1, keepdims=True) + epsilon
    )
    normed_own = (scaled * norm_gain).astype(jnp.bfloat16)
    normed = lax.all_gather(normed_own, ("fs", "tp"), axis=0, tiled=True)
    block_rows = normed.shape[0]
    channels = w_conv_post.shape[1]
    head_dim = w_key.shape[1]
    local_heads = w_query.shape[1] // head_dim
    group = lax.axis_index(("fs", "tp"))
    local_weight = jnp.concatenate([w_conv_post, w_conv_pre, w_conv_value, w_query], axis=1)
    projected = jnp.dot(normed, local_weight, preferred_element_type=jnp.float32).astype(
        jnp.bfloat16
    )
    post_gate = projected[:, :channels]
    pre_gate = projected[:, channels : 2 * channels]
    conv_value = projected[:, 2 * channels : 3 * channels]
    queries = projected[:, 3 * channels :].reshape(block_rows, local_heads, head_dim)
    mixed_in = (pre_gate.astype(jnp.float32) * conv_value.astype(jnp.float32)).astype(jnp.bfloat16)
    kernel = conv_taps.shape[0]
    carried = passed_along(mixed_in[block_rows - (kernel - 1) :], "sp", 1)
    extended = jnp.concatenate([carried, mixed_in], axis=0).astype(jnp.float32)
    tap_weights = lax.dynamic_slice_in_dim(conv_taps, group * channels, channels, 1).astype(
        jnp.float32
    )
    conv_sum = tap_weights[0] * extended[0:block_rows]
    for offset in range(1, kernel):
        conv_sum = conv_sum + tap_weights[offset] * extended[offset : offset + block_rows]
    conv_out = (post_gate.astype(jnp.float32) * conv_sum).astype(jnp.bfloat16)
    core_index = lax.axis_index("tp")
    half_rows = block_rows // 2
    own_rows = lax.dynamic_slice_in_dim(normed, core_index * half_rows, half_rows, 0)
    pair_weight = jnp.concatenate([w_key, w_value], axis=1)
    pair_rows = jnp.dot(own_rows, pair_weight, preferred_element_type=jnp.float32).astype(
        jnp.bfloat16
    )
    key_half = pair_rows[:, :head_dim]
    value_half = pair_rows[:, head_dim:]
    head_gates = lax.dynamic_slice_in_dim(log_gate_cache, group * local_heads, local_heads, 0)
    anchor = lax.axis_index("sp") * block_rows
    gate_query = lax.dynamic_slice_in_dim(head_gates, anchor, block_rows, 1).T
    sequence_places = anchor + lax.iota(jnp.int32, block_rows)
    score_scale = head_dim ** (-0.5)

    def absorb(carried_state, key_block, value_block, sub_start):
        running_max, running_sum, weighted = carried_state
        sub_width = key_block.shape[0]
        scores = (
            jnp.einsum("qhd,kd->qhk", queries, key_block, preferred_element_type=jnp.float32)
            * score_scale
        )
        gate_keys = lax.dynamic_slice_in_dim(head_gates, sub_start, sub_width, 1)
        scores = scores + gate_query[:, :, None] - gate_keys[None, :, :]
        key_positions = sub_start + lax.iota(jnp.int32, sub_width)
        scores = jnp.where(
            sequence_places[:, None, None] >= key_positions[None, None, :], scores, masked_score
        )
        new_max = jnp.maximum(running_max, jnp.max(scores, axis=2))
        rescale = jnp.exp(running_max - new_max)
        weights = jnp.exp(scores - new_max[:, :, None])
        running_sum = running_sum * rescale + jnp.sum(weights, axis=2)
        weighted = weighted * rescale[:, :, None] + jnp.einsum(
            "qhk,kd->qhd",
            weights.astype(jnp.bfloat16),
            value_block,
            preferred_element_type=jnp.float32,
        )
        return (new_max, running_sum, weighted)

    initial = (
        jnp.full((block_rows, local_heads), masked_score, jnp.float32),
        jnp.zeros((block_rows, local_heads), jnp.float32),
        jnp.zeros((block_rows, local_heads, head_dim), jnp.float32),
    )
    key_piece = lax.all_gather(key_half, ("sp", "tp"), axis=0, tiled=True)
    value_piece = lax.all_gather(value_half, ("sp", "tp"), axis=0, tiled=True)
    key_count = key_piece.shape[0]
    sub_width = 512

    def sweep_keys(current):

        def absorb_step(running, step_index):
            sub_start = step_index * sub_width
            key_block = lax.dynamic_slice_in_dim(key_piece, sub_start, sub_width, 0)
            value_block = lax.dynamic_slice_in_dim(value_piece, sub_start, sub_width, 0)
            return (absorb(running, key_block, value_block, sub_start), None)

        result, unused = lax.scan(
            absorb_step, current, jnp.arange(key_count // sub_width, dtype=jnp.int32)
        )
        return result

    def keep_state(current):
        return current

    running_max, running_sum, weighted = lax.cond(
        jnp.int32(0) <= anchor + block_rows - 1, sweep_keys, keep_state, initial
    )
    attn_out = (
        (weighted / running_sum[:, :, None])
        .astype(jnp.bfloat16)
        .reshape(block_rows, local_heads * head_dim)
    )
    return lax.psum_scatter(
        (
            jnp.dot(conv_out, w_out_conv, preferred_element_type=jnp.float32)
            + jnp.dot(attn_out, w_out_attn, preferred_element_type=jnp.float32)
        ).astype(jnp.bfloat16),
        ("fs", "tp"),
        scatter_dimension=0,
        tiled=True,
    )


def solution(mesh):
    placed = (
        P(("sp", "fs", "tp"), None),
        P(),
        P(None, ("fs", "tp")),
        P(None, "fs"),
        P(None, "fs"),
        P(None, ("fs", "tp")),
        P(None, ("fs", "tp")),
        P(None, ("fs", "tp")),
        P(),
        P(),
        P(("fs", "tp"), None),
        P(("fs", "tp"), None),
    )
    return jax.shard_map(
        shards, mesh=mesh, in_specs=placed, out_specs=P(("sp", "fs", "tp"), None), check_vma=False
    )
```

profile of v0, /device:TPU:16, one launch (start us, length us, event | category | flops | bytes accessed | tf_op | source)
XLA Modules:
  0.0 121.7 jit_solution(4051089183334472649)
XLA Ops:
  6.5 0.0 copy-start
  6.5 0.0 copy-start.2
  6.5 0.0 all-gather.2.cloned.1.call-start
  6.5 1.2 fusion.32
  7.7 1.7 %fusion.34 = bf16[32,2048]{1,0:T(8,128)(2,1)} fusion(bf16[32,2048]{1,0:T(8,128)(2,1)} %param.16, f32[2048]{0:T(1024)} %param.17, f32[32]{0:T(128)S(1)} %add_rsqrt_fusion), kind=kLoop, calls=%fused_computation.47 | loop fusion | flops 262144 | bytes 270464 | tf_op jit(solution)/shard_map/convert_element_type | solution.py:34
  9.4 0.0 all-gather.2.cloned.1.call-update
  9.4 0.0 reduce-scatter.2.cloned.1.call-start
  9.5 0.7 dynamic-slice_convert_fusion
  10.2 0.8 dynamic-slice_bitcast_fusion
  11.0 23.0 %all-gather.2.cloned.1.call-done = bf16[256,2048]{1,0:T(8,128)(2,1)} async-done(((bf16[32,2048]{1,0:T(8,128)(2,1)}), bf16[256,2048]{1,0:T(8,128)(2,1)}) %all-gather.2.cloned.1.call-update) | async-done | bytes 1048592 | tf_op jit(solution)/shard_map/all_gather | solution.py:35
  34.0 0.0 copy-start.3
  34.0 0.0 copy-start.4
  34.0 1.8 %convolution_convert_fusion = bf16[128,256]{1,0:T(8,128)(2,1)S(1)} fusion(bf16[2048,128]{1,0:T(8,128)(2,1)} %param.20, bf16[2048,128]{1,0:T(8,128)(2,1)} %param.19, bf16[256,2048]{1,0:T(8,128)(2,1)} %all-gather.2.cloned.1.call-done, s32[]{:T(128)S(6)} %select_n.27), kind=kOutput, calls=%fused_computation.38 | convolution fusion | flops 136347648 | bytes 1638404 | tf_op jit(solution)/shard_map/dot_general | solution.py:64
  35.8 0.0 copy-done.2
  35.8 0.0 copy-done.3
  35.9 0.0 copy-done.4
  35.9 2.2 %fusion.25 = bf16[256,640]{1,0:T(8,128)(2,1)S(1)} fusion(bf16[256,2048]{1,0:T(8,128)(2,1)S(1)} %copy-done.3, bf16[2048,256]{1,0:T(8,128)(2,1)S(1)} %copy-done.2, bf16[2048,128]{1,0:T(8,128)(2,1)S(1)} %copy-done.4, bf16[2048,128]{1,0:T(8,128)(2,1)} %param.22, bf16[2048,128]{1,0:T(8,128)(2,1)} %param.23), kind=kOutput, calls=%fused_computation.37 | convolution fusion | flops 681738240 | bytes 3997696 | tf_op jit(solution)/shard_map/dot_general | solution.py:42
  38.1 3.4 %collective-permute-start = (bf16[2,128]{1,0:T(2,128)(2,1)S(1)}, bf16[2,128]{1,0:T(2,128)(2,1)S(1)}, u32[]{:S(2)}, u32[]{:S(2)}) collective-permute-start(bf16[2,128]{1,0:T(2,128)(2,1)S(1)} %slice.57), channel_id=1, source_target_pairs={{0,8},{8,16},{16,24},{1,9},{9,17},{17,25},{2,10},{10,18},{18,26},{... | collective-permute-start | bytes 1544 | tf_op jit(solution)/shard_map/ppermute | solution.py:13
  41.5 12.4 %all_gather.11 = bf16[1024,128]{1,0:T(8,128)(2,1)S(1)} all-gather(bf16[128,128]{1,0:T(8,128)(2,1)S(1)} %get-tuple-element.195), channel_id=1, replica_groups=mesh['sp'=4,'fs'=4,'tp'=2] {'sp','tp'}, dimensions={0}, use_global_device_ids=true | all-gather | bytes 294912 | tf_op jit(solution)/shard_map/all_gather | solution.py:106
  54.0 14.2 %all_gather.10 = bf16[1024,128]{1,0:T(8,128)(2,1)S(1)} all-gather(bf16[128,128]{1,0:T(8,128)(2,1)S(1)} %get-tuple-element.196), channel_id=1, replica_groups=mesh['sp'=4,'fs'=4,'tp'=2] {'sp','tp'}, dimensions={0}, use_global_device_ids=true | all-gather | bytes 294912 | tf_op jit(solution)/shard_map/all_gather | solution.py:105
  68.1 0.0 copy-start.1
  68.1 7.9 %conditional.1 = (f32[256,2]{0,1:T(2,128)}, f32[256,2,128]{0,2,1:T(8,128)S(1)}) conditional(s32[]{:T(128)} %convert_element_type.55, () %tuple.19, (bf16[256,640]{1,0:T(8,128)(2,1)S(1)}, f32[16,1024]{1,0:T(8,128)}, s32[]{:T(128)}, s32[]{:T(128)}, s32[256]{0:T(256)S(1)}, /*index=5*/bf16[1024,128]{1,0:T(8,128)(2,1)S(1)}, f32[256,2]{0,1:T(2,128)S(1)}, ...), branch_computations={%region_1.0_spmd, %region_2.7_spmd} | conditional | flops 136908032 | bytes 6100363 | solution.py:126
  68.2 0.9 constant_dynamic-slice_fusion.1
  69.1 0.2 copy.16
  69.3 0.1 copy.15
  69.4 6.5 %while.18 = (s32[]{:T(128)}, f32[256,2]{0,1:T(2,128)S(1)}, f32[256,2]{0,1:T(2,128)}, f32[256,2,128]{2,0,1:T(8,128)S(1)}, s32[256]{0:T(256)S(1)}, /*index=5*/s32[...) while((s32[]{:T(128)}, f32[256,2]{0,1:T(2,128)S(1)}, ...), condition=%wide.region_6.6_spmd.clone, body=%wide.region_3.5_spmd.clone.sunk | while | flops 136907776 | bytes 4377835 | solution.py:118
  69.4 0.6 dynamic_slice.58
  70.6 0.1 broadcast_compare_fusion.2
  70.8 0.4 fusion.65
  71.2 0.2 fusion.67
  71.3 0.6 fusion.68
  71.9 0.4 convolution_add_fusion.3
  72.3 0.6 dynamic_slice.58
  73.5 0.1 broadcast_compare_fusion.2
  73.7 0.4 fusion.65
  74.1 0.2 fusion.67
  74.2 1.3 %fusion.68 = (f32[256,2]{0,1:T(2,128)}, f32[256,2]{0,1:T(2,128)S(1)}) fusion(f32[256,2]{0,1:T(2,128)S(1)} %fusion.67, f32[256,2]{0,1:T(2,128)} %get-tuple-element.292, pred[]{:T(512)S(6)} %compare.3, f32[256,2]{0,1:T(2,128)S(1)} %fusion.66, f32[256,2]{0,1:T(2,128)S(1)} %get-tuple-element.291), kind=kLoop, calls=%fused_computation.17.clone.1 | loop fusion | flops 2560 | bytes 12289 | tf_op jit(solution)/shard_map/cond/branch_1_fun/while/body/eval_jaxpr/add | solution.py:91
  75.5 0.4 convolution_add_fusion.3
  75.9 0.1 copy.20
  76.0 0.7 divide_convert_fusion
  76.7 0.0 collective-permute-done
  76.8 0.0 copy-done.1
  76.8 0.4 fusion.39
  77.2 0.0 copy-done
  77.2 1.4 %fusion.24 = bf16[256,2048]{1,0:T(8,128)(2,1)} fusion(f32[256,2048]{1,0:T(8,128)S(1)} %fusion.39, bf16[256,256]{0,1:T(8,128)(2,1)S(1)} %bitcast.38, bf16[256,2048]{1,0:T(8,128)(2,1)S(1)} %copy-done), kind=kOutput, calls=%fused_computation.36 | convolution fusion | flops 269484032 | bytes 4325376 | tf_op jit(solution)/shard_map/dot_general | solution.py:137
  78.7 0.0 reduce-scatter.2.cloned.1.call-update
  78.7 36.2 %reduce-scatter.2.cloned.1.call-done = bf16[32,2048]{1,0:T(8,128)(2,1)} async-done(((bf16[256,2048]{1,0:T(8,128)(2,1)}), bf16[32,2048]{1,0:T(8,128)(2,1)}) %reduce-scatter.2.cloned.1.call-update) | async-done | bytes 131088 | tf_op jit(solution)/shard_map/reduce_scatter | solution.py:134
  (21 shorter events, 0.1 us)
Async XLA Ops:
  6.5 70.7 %copy-start = (bf16[256,2048]{1,0:T(8,128)(2,1)S(1)}, bf16[256,2048]{1,0:T(8,128)(2,1)}, u32[]{:S(2)}) copy-start(bf16[256,2048]{1,0:T(8,128)(2,1)} %param.27) | copy-start | bytes 3145732
  6.5 29.3 %copy-start.2 = (bf16[2048,256]{1,0:T(8,128)(2,1)S(1)}, bf16[2048,256]{1,0:T(8,128)(2,1)}, u32[]{:S(2)}) copy-start(bf16[2048,256]{1,0:T(8,128)(2,1)} %param.18) | copy-start | bytes 3145732
  6.5 27.5 %all-gather.2.cloned.1.call-start = ((), (), s32[]{:S(2)}) async-start(), calls=%async_computation.1 | async-start | bytes 1179648 | tf_op jit(solution)/shard_map/all_gather | solution.py:35
  9.4 105.5 %reduce-scatter.2.cloned.1.call-start = ((), (), s32[]{:S(2)}) async-start(), calls=%async_computation.2 | async-start | bytes 1179648 | tf_op jit(solution)/shard_map/reduce_scatter | solution.py:134
  34.0 1.8 %copy-start.3 = (bf16[256,2048]{1,0:T(8,128)(2,1)S(1)}, bf16[256,2048]{1,0:T(8,128)(2,1)}, u32[]{:S(2)}) copy-start(bf16[256,2048]{1,0:T(8,128)(2,1)} %all-gather.2.cloned.1.call-done) | copy-start | bytes 3145732
  34.0 1.8 %copy-start.4 = (bf16[2048,128]{1,0:T(8,128)(2,1)S(1)}, bf16[2048,128]{1,0:T(8,128)(2,1)}, u32[]{:S(2)}) copy-start(bf16[2048,128]{1,0:T(8,128)(2,1)} %param.21) | copy-start | bytes 1572868
  38.1 38.6 %collective-permute-start = (bf16[2,128]{1,0:T(2,128)(2,1)S(1)}, bf16[2,128]{1,0:T(2,128)(2,1)S(1)}, u32[]{:S(2)}, u32[]{:S(2)}) collective-permute-start(bf16[2,128]{1,0:T(2,128)(2,1)S(1)} %slice.57), channel_id=1, source_target_pairs={{0,8},{8,16},{16,24},{1,9},{9,17},{17,25},{2,10},{10,18},{18,26},{... | collective-permute-start | bytes 1544 | tf_op jit(solution)/shard_map/ppermute | solution.py:13
  68.1 8.6 %copy-start.1 = (bf16[128,2048]{1,0:T(8,128)(2,1)S(1)}, bf16[128,2048]{1,0:T(8,128)(2,1)}, u32[]{:S(2)}) copy-start(bf16[128,2048]{1,0:T(8,128)(2,1)} %param.26) | copy-start | bytes 1572868
Sparse Core Ops, SparseCore 0:
  9.6 24.4 all-gather.1
  78.8 36.0 reduce-scatter.1
where the time goes:
time: 124 us; the launch traced here: 122 us
  waiting for transfers between devices  59.3 us (48%)
  blocking collectives  26.6 us (21%)
  between operations  13.5 us (11%)
  matrix products  7.39 us (6%)
  other arithmetic  6.81 us (5%)
  starting transfers between devices  3.44 us (3%)
  local copies, waits for them, and re-layouts  3.38 us (3%)
  loops' own time  1.32 us (1%)
    reduce_scatter x1, waiting for transfers between devices, shards(): lax.psum_scatter((jnp.dot(conv_out, w_out_conv, preferred_element_type=jn...  36.2 us
    all_gather x1, waiting for transfers between devices, shards(): normed = lax.all_gather(normed_own, ('fs', 'tp'), axis=0, tiled=True)  23 us
    all_gather x1, blocking collectives, shards(): key_piece = lax.all_gather(key_half, ('sp', 'tp'), axis=0, tiled=True)  14.2 us
    all_gather x1, blocking collectives, shards(): value_piece = lax.all_gather(value_half, ('sp', 'tp'), axis=0, tiled=True)  12.4 us
    ppermute x1, starting transfers between devices, passed_along(): return lax.ppermute(block, axis, route)  3.39 us
  transfers between devices with their start and end apart: 3, of which 2 were waited for; matrix products, arithmetic and copies ran while one was open for 7% of the time, Pallas kernels for 0%

commit v1 on v0

v1 whole, which is shorter than its diff:
```python
import functools

import jax
import jax.numpy as jnp
from jax import lax
from jax.experimental import pallas as pl
from jax.experimental.pallas import tpu as pltpu
from jax.sharding import PartitionSpec as P

epsilon = 1e-06
masked_score = -1e30
MESH = pl.DeviceIdType.MESH
f32 = jnp.float32
bf16 = jnp.bfloat16


def dot(a, b):
    return jnp.dot(a, b, preferred_element_type=f32)


def layer_kernel(
    n_sp,
    n_fs,
    n_tp,
    col_chunk,
    tokens,
    gain,
    w_query,
    w_key,
    w_value,
    w_conv_value,
    w_conv_pre,
    w_conv_post,
    taps,
    gates,
    w_out_conv,
    w_out_attn,
    out,
    normed,
    kv_w,
    pair_w,
    rest_w,
    out_w,
    kv,
    ext,
    tail,
    halo,
    post_buf,
    q_buf,
    gate_col,
    run_max,
    run_sum,
    acc,
    mix_in,
    part,
    sib_in,
    pair_sum,
    rs_in,
    w_sem,
    ag_send,
    ag_recv,
    agf_send,
    agf_recv,
    kv_send,
    kv_recv,
    kvf_send,
    kvf_recv,
    halo_send,
    halo_recv,
    sib_send,
    sib_recv,
    rs_send,
    rs_recv,
):
    s = lax.axis_index("sp")
    f = lax.axis_index("fs")
    t = lax.axis_index("tp")
    g = f * n_tp + t
    own_rows, width = tokens.shape
    block = own_rows * n_fs * n_tp
    channels = w_conv_post.shape[1]
    head_dim = w_key.shape[1]
    heads = w_query.shape[1] // head_dim
    half = block // n_tp
    scale = head_dim ** (-0.5)

    def rc(src, dst, send, recv, device):
        return pltpu.make_async_remote_copy(
            src_ref=src,
            dst_ref=dst,
            send_sem=send,
            recv_sem=recv,
            device_id=device,
            device_id_type=MESH,
        )

    def fs_peer(df):
        return (s, lax.rem(f + df, n_fs), t)

    def tp_peer(dt):
        return (s, f, lax.rem(t + dt, n_tp))

    barrier = pltpu.get_barrier_semaphore()
    for dt in range(1, n_tp):
        pl.semaphore_signal(barrier, inc=1, device_id=tp_peer(dt), device_id_type=MESH)
    for df in range(1, n_fs):
        pl.semaphore_signal(barrier, inc=1, device_id=fs_peer(df), device_id_type=MESH)

    def greet(ds, c):
        pl.semaphore_signal(
            barrier, inc=1, device_id=(lax.rem(s + ds, n_sp), f, t), device_id_type=MESH
        )
        return c

    lax.fori_loop(1, n_sp, greet, 0)

    c0, c1, hd = channels, 2 * channels, head_dim
    qw = w_query.shape[1]
    loads = [
        (w_key, kv_w.at[:, 0:hd]),
        (w_value, kv_w.at[:, hd : 2 * hd]),
        (w_conv_pre, pair_w.at[:, 0:c0]),
        (w_conv_value, pair_w.at[:, c0:c1]),
        (w_query, rest_w.at[:, 0:qw]),
        (w_conv_post, rest_w.at[:, qw : qw + channels]),
        (w_out_conv, out_w.at[0:channels, :]),
        (w_out_attn, out_w.at[channels : channels + qw, :]),
    ]
    load_copies = [
        pltpu.make_async_copy(src, dst, w_sem.at[i]) for i, (src, dst) in enumerate(loads)
    ]
    for cp in load_copies:
        cp.start()

    rows = tokens[...].astype(f32)
    inv = lax.rsqrt(jnp.mean(rows * rows, axis=1, keepdims=True) + epsilon)
    normed[pl.ds(pl.multiple_of(g * own_rows, own_rows), own_rows), :] = (
        rows * inv * gain[...]
    ).astype(bf16)

    pl.semaphore_wait(barrier, (n_tp - 1) + (n_fs - 1) + (n_sp - 1))

    def slot(fi, ti):
        return normed.at[pl.ds(pl.multiple_of((fi * n_tp + ti) * own_rows, own_rows), own_rows), :]

    def ag_copy(df):
        return rc(slot(f, t), slot(f, t), ag_send.at[df], ag_recv.at[df], fs_peer(df))

    def agf_copy(df, dt):
        origin = lax.rem(f - df + n_fs, n_fs)
        i = df * n_tp + dt
        return rc(slot(origin, t), slot(origin, t), agf_send.at[i], agf_recv.at[i], tp_peer(dt))

    for df in range(1, n_fs):
        ag_copy(df).start()
    for dt in range(1, n_tp):
        agf_copy(0, dt).start()

    for h in range(heads):
        row = gates[pl.ds(g * heads + h, 1), pl.ds(pl.multiple_of(s * block, 128), block)]
        gate_col[h] = jnp.broadcast_to(row, (128, block)).T

    for df in range(1, n_fs):
        ag_copy(df).wait_recv()
        for dt in range(1, n_tp):
            agf_copy(df, dt).start()
    for df in range(n_fs):
        for dt in range(1, n_tp):
            agf_copy(df, dt).wait_recv()

    load_copies[0].wait()
    load_copies[1].wait()
    base = pl.multiple_of(s * block, block)
    kv[pl.ds(base, block), :] = dot(normed[...], kv_w[...]).astype(bf16)

    def kv_piece(si, ti):
        return kv.at[pl.ds(pl.multiple_of(si * block + ti * half, half), half), :]

    def kv_copy(ds, origin, dest):
        return rc(
            kv_piece(origin, t), kv_piece(origin, t), kv_send.at[ds], kv_recv.at[ds], (dest, f, t)
        )

    def send_kv(ds, c):
        kv_copy(ds, s, s + ds).start()
        return c

    lax.fori_loop(1, n_sp - s, send_kv, 0)

    load_copies[2].wait()
    load_copies[3].wait()
    pair = dot(normed[...], pair_w[...]).astype(bf16)
    mixed_in = (pair[:, :c0].astype(f32) * pair[:, c0:].astype(f32)).astype(bf16)
    tail[...] = mixed_in[block - 16 :, :]
    ext[pl.ds(8, block), :] = mixed_in.astype(f32)

    def halo_copy(dest):
        return rc(tail, halo, halo_send, halo_recv, (dest, f, t))

    @pl.when(s + 1 < n_sp)
    def _():
        halo_copy(s + 1).start()

    @pl.when(s == 0)
    def _():
        halo[...] = jnp.zeros_like(halo)

    load_copies[4].wait()
    load_copies[5].wait()
    rest = dot(normed[...], rest_w[...]).astype(bf16)
    for h in range(heads):
        q_buf[h] = rest[:, h * hd : (h + 1) * hd]
    post_buf[...] = rest[:, qw:]

    def absorb(si, first):
        start = pl.multiple_of(si * block, block)
        key_block = kv[pl.ds(start, block), 0:hd]
        value_block = kv[pl.ds(start, block), hd : 2 * hd]
        for h in range(heads):
            scores = (
                lax.dot_general(
                    q_buf[h], key_block, (((1,), (1,)), ((), ())), preferred_element_type=f32
                )
                * scale
            )
            gate_row = gates[pl.ds(g * heads + h, 1), pl.ds(start, block)]
            scores = scores + gate_col[h][:, 0:1] - gate_row
            if first:
                q_pos = lax.broadcasted_iota(jnp.int32, (block, block), 0)
                k_pos = lax.broadcasted_iota(jnp.int32, (block, block), 1)
                scores = jnp.where(q_pos >= k_pos, scores, masked_score)
                new_max = jnp.max(scores, axis=1, keepdims=True)
                weights = jnp.exp(scores - new_max)
                run_sum[h] = jnp.broadcast_to(jnp.sum(weights, axis=1, keepdims=True), (block, 128))
                run_max[h] = jnp.broadcast_to(new_max, (block, 128))
                acc[h] = dot(weights.astype(bf16), value_block)
            else:
                old_max = run_max[h][:, 0:1]
                new_max = jnp.maximum(old_max, jnp.max(scores, axis=1, keepdims=True))
                rescale = jnp.exp(old_max - new_max)
                weights = jnp.exp(scores - new_max)
                run_sum[h] = run_sum[h] * rescale + jnp.sum(weights, axis=1, keepdims=True)
                run_max[h] = jnp.broadcast_to(new_max, (block, 128))
                acc[h] = acc[h] * rescale + dot(weights.astype(bf16), value_block)

    absorb(s, True)

    @pl.when(s > 0)
    def _():
        halo_copy(s).wait_recv()

    ext[pl.ds(0, 8), :] = halo[...].astype(f32)[8:, :]
    tap = taps[:, pl.ds(pl.multiple_of(g * channels, channels), channels)].astype(f32)
    count = taps.shape[0]
    conv_sum = tap[0:1] * ext[pl.ds(8 - count + 1, block), :]
    for i in range(1, count):
        conv_sum = conv_sum + tap[i : i + 1] * ext[pl.ds(8 - count + 1 + i, block), :]
    mix_in[:, 0:channels] = (post_buf[...].astype(f32) * conv_sum).astype(bf16)

    def kvf_copy(ds, dt):
        i = ds * n_tp + dt
        return rc(
            kv_piece(s - ds, t), kv_piece(s - ds, t), kvf_send.at[i], kvf_recv.at[i], tp_peer(dt)
        )

    def pass_on(ds):
        kv_copy(ds, s - ds, s).wait_recv()
        for dt in range(1, n_tp):
            kvf_copy(ds, dt).start()

    @pl.when(s > 0)
    def _():
        pass_on(1)

    def earlier(ds, c):
        @pl.when(ds < s)
        def _():
            pass_on(ds + 1)

        for dt in range(1, n_tp):
            kvf_copy(ds, dt).wait_recv()
        absorb(s - ds, False)
        return c

    lax.fori_loop(1, s + 1, earlier, 0)
    for h in range(heads):
        mix_in[:, channels + h * hd : channels + (h + 1) * hd] = (
            acc[h] / run_sum[h][:, 0:1]
        ).astype(bf16)

    load_copies[6].wait()
    load_copies[7].wait()
    n_chunks = width // col_chunk

    def cols(c):
        return slice(c * col_chunk, (c + 1) * col_chunk)

    def sib_copy(c, dt):
        i = c * n_tp + dt
        return rc(
            part.at[lax.rem(t + dt, n_tp), :, cols(c)],
            sib_in.at[dt, :, cols(c)],
            sib_send.at[i],
            sib_recv.at[i],
            tp_peer(dt),
        )

    def rs_copy(c, df):
        i = c * n_fs + df
        dest = lax.rem(f + df, n_fs)
        return rc(
            pair_sum.at[pl.ds(pl.multiple_of(dest * own_rows, own_rows), own_rows), cols(c)],
            rs_in.at[df, :, cols(c)],
            rs_send.at[i],
            rs_recv.at[i],
            fs_peer(df),
        )

    for c in range(n_chunks):
        piece = dot(mix_in[...], out_w[:, cols(c)]).astype(bf16)
        for fi in range(n_fs):
            for ti in range(n_tp):
                r = (fi * n_tp + ti) * own_rows
                part[ti, fi * own_rows : (fi + 1) * own_rows, cols(c)] = piece[r : r + own_rows]
        for dt in range(1, n_tp):
            sib_copy(c, dt).start()

    for c in range(n_chunks):
        total = part[t, :, cols(c)].astype(f32)
        for dt in range(1, n_tp):
            sib_copy(c, dt).wait_recv()
            total = total + sib_in[dt, :, cols(c)].astype(f32)
        pair_sum[:, cols(c)] = total.astype(bf16)
        for df in range(1, n_fs):
            rs_copy(c, df).start()

    own = pl.ds(pl.multiple_of(f * own_rows, own_rows), own_rows)
    for c in range(n_chunks):
        total = pair_sum[own, cols(c)].astype(f32)
        for df in range(1, n_fs):
            rs_copy(c, df).wait_recv()
            total = total + rs_in[df, :, cols(c)].astype(f32)
        out[:, cols(c)] = total.astype(bf16)

    for df in range(1, n_fs):
        ag_copy(df).wait_send()
    for df in range(n_fs):
        for dt in range(1, n_tp):
            agf_copy(df, dt).wait_send()

    def kv_left(ds, c):
        kv_copy(ds, s, s + ds).wait_send()
        return c

    lax.fori_loop(1, n_sp - s, kv_left, 0)

    def kvf_left(ds, c):
        for dt in range(1, n_tp):
            kvf_copy(ds, dt).wait_send()
        return c

    lax.fori_loop(1, s + 1, kvf_left, 0)

    @pl.when(s + 1 < n_sp)
    def _():
        halo_copy(s + 1).wait_send()

    for c in range(n_chunks):
        for dt in range(1, n_tp):
            sib_copy(c, dt).wait_send()
        for df in range(1, n_fs):
            rs_copy(c, df).wait_send()


def solution(mesh):
    n_sp, n_fs, n_tp = (mesh.shape[a] for a in ("sp", "fs", "tp"))

    def shards(
        tokens,
        norm_gain,
        w_query,
        w_key,
        w_value,
        w_conv_value,
        w_conv_pre,
        w_conv_post,
        conv_taps,
        log_gate_cache,
        w_out_conv,
        w_out_attn,
    ):
        own_rows, width = tokens.shape
        block = own_rows * n_fs * n_tp
        channels = w_conv_post.shape[1]
        head_dim = w_key.shape[1]
        qw = w_query.shape[1]
        heads = qw // head_dim
        col_chunk = 512
        n_chunks = width // col_chunk
        vm = pl.BlockSpec(memory_space=pltpu.VMEM)
        hbm = pl.BlockSpec(memory_space=pl.ANY)
        V = pltpu.VMEM
        D = pltpu.SemaphoreType.DMA
        return pl.pallas_call(
            functools.partial(layer_kernel, n_sp, n_fs, n_tp, col_chunk),
            out_shape=jax.ShapeDtypeStruct((own_rows, width), bf16),
            in_specs=[vm, vm] + [hbm] * 6 + [vm, vm] + [hbm] * 2,
            out_specs=vm,
            scratch_shapes=[
                V((block, width), bf16),
                V((width, 2 * head_dim), bf16),
                V((width, 2 * channels), bf16),
                V((width, qw + channels), bf16),
                V((channels + qw, width), bf16),
                V((n_sp * block, 2 * head_dim), bf16),
                V((block + 8, channels), f32),
                V((16, channels), bf16),
                V((16, channels), bf16),
                V((block, channels), bf16),
                V((heads, block, head_dim), bf16),
                V((heads, block, 128), f32),
                V((heads, block, 128), f32),
                V((heads, block, 128), f32),
                V((heads, block, head_dim), f32),
                V((block, channels + qw), bf16),
                V((n_tp, n_fs * own_rows, width), bf16),
                V((n_tp, n_fs * own_rows, width), bf16),
                V((n_fs * own_rows, width), bf16),
                V((n_fs, own_rows, width), bf16),
                D((8,)),
                D((n_fs,)),
                D((n_fs,)),
                D((n_fs * n_tp,)),
                D((n_fs * n_tp,)),
                D((n_sp,)),
                D((n_sp,)),
                D((n_sp * n_tp,)),
                D((n_sp * n_tp,)),
                D,
                D,
                D((n_chunks * n_tp,)),
                D((n_chunks * n_tp,)),
                D((n_chunks * n_fs,)),
                D((n_chunks * n_fs,)),
            ],
            compiler_params=pltpu.CompilerParams(
                collective_id=0, has_side_effects=True, vmem_limit_bytes=60 * 1024 * 1024
            ),
        )(
            tokens,
            norm_gain.reshape(1, width),
            w_query,
            w_key,
            w_value,
            w_conv_value,
            w_conv_pre,
            w_conv_post,
            conv_taps,
            log_gate_cache,
            w_out_conv,
            w_out_attn,
        )

    placed = (
        P(("sp", "fs", "tp"), None),
        P(),
        P(None, ("fs", "tp")),
        P(None, "fs"),
        P(None, "fs"),
        P(None, ("fs", "tp")),
        P(None, ("fs", "tp")),
        P(None, ("fs", "tp")),
        P(),
        P(),
        P(("fs", "tp"), None),
        P(("fs", "tp"), None),
    )
    return jax.shard_map(
        shards, mesh=mesh, in_specs=placed, out_specs=P(("sp", "fs", "tp"), None), check_vma=False
    )
```

time: 124 us -> 35.3 us (0.28); the launches traced: 122 us -> 34.9 us
  waiting for transfers between devices: 59.3 us -> 0 us
  Pallas kernels: 0 us -> 33.4 us
  blocking collectives: 26.6 us -> 0 us
  between operations: 13.5 us -> 0.01 us
  matrix products: 7.39 us -> 0 us
  other arithmetic: 6.81 us -> 0 us
  starting transfers between devices: 3.44 us -> 0 us
  local copies, waits for them, and re-layouts: 3.38 us -> 1.57 us
  loops' own time: 1.32 us -> 0 us
    reduce_scatter x1 -> x0, waiting for transfers between devices: 36.2 us -> none  [shards(): lax.psum_scatter((jnp.dot(conv_out, w_out_conv, preferred_element_type=jn...]
    pallas_call x0 -> x1, Pallas kernels: none -> 33.4 us  [shards(): pl.pallas_call(functools.partial(layer_kernel, n_sp, n_fs, n_tp, col_chun...]
    all_gather x2 -> x0, blocking collectives: 26.6 us -> none  [the longest x1 14.2 us: shards(): key_piece = lax.all_gather(key_half, ('sp', 'tp'), axis=0, tiled=True)]
    all_gather x1 -> x0, waiting for transfers between devices: 23 us -> none  [shards(): normed = lax.all_gather(normed_own, ('fs', 'tp'), axis=0, tiled=True)]
    dot_general x8 -> x0, matrix products: 7.39 us -> none  [the longest x1 2.23 us: shards(): jnp.dot(normed, local_weight, preferred_element_type=jnp.float32)]
    ppermute x1 -> x0, starting transfers between devices: 3.39 us -> none  [passed_along(): return lax.ppermute(block, axis, route)]
    convert_element_type x5 -> x0, other arithmetic: 3.1 us -> none  [the longest x1 1.67 us: shards(): normed_own = (scaled * norm_gain).astype(jnp.bfloat16)]
    dynamic_slice x5 -> x0, local copies, waits for them, and re-layouts: 2.09 us -> none  [the longest x2 1.16 us: sweep_keys(): lax.scan(absorb_step, current, jnp.arange(key_count // sub_width, dtype=j...]
  transfers between devices with their start and end apart: 3 -> 0, of which waited for: 2 -> 0; matrix products, arithmetic and copies ran while one was open for 7% -> 0% of each run, Pallas kernels for 0% -> 0%
where the time goes in v1:
time: 35.3 us; the launch traced here: 34.9 us
  Pallas kernels  33.4 us (95%)
  local copies, waits for them, and re-layouts  1.57 us (4%)
    pallas_call x1, Pallas kernels, shards(): pl.pallas_call(functools.partial(layer_kernel, n_sp, n_fs, n_tp, col_chun...  33.4 us
    unnamed x1, local copies, waits for them, and re-layouts  1.57 us

profile of v1, /device:TPU:16, one launch (start us, length us, event | category | flops | bytes accessed | tf_op | source)
XLA Modules:
  0.0 34.9 jit_solution(18359357543973909093)
XLA Ops:
  0.0 33.4 %shard_map.118 = bf16[32,2048]{1,0:T(8,128)(2,1)} custom-call(bf16[32,2048]{1,0:T(8,128)(2,1)} %tokens.1, f32[1,2048]{1,0:T(1,128)} %bitcast.1, bf16[2048,256]{1,0:T(8,128)(2,1)} %w_query.1, bf16[2048,128]{1,0:T(8,128)(2,1)} %w_key.1, bf16[2048,128]{1,0:T(8,128)(2,1)} %w_value.1, bf16[2048,128]{1,0:T(8,128)(2,1)} %w_conv_value.1, ...), custom_call_target="tpu_custom_call" | custom-call | tf_op jit(solution)/shard_map/pallas_call | solution.py:404
  33.4 1.6 %copy.14 = bf16[32,2048]{1,0:T(8,128)(2,1)} copy(bf16[32,2048]{1,0:T(8,128)(2,1)} %shard_map.118) | data formatting | bytes 262144
